TPU v7x, 32 devices: a whole 2x2x4 slice. The times are simulated.
32 devices in a mesh: sp: 8 (over z, y), tp: 4 (over x, core).
Axes of the slice: x: 2, y: 2, z: 4, core: 2. Of those that a mesh axis runs over, the one named last changes fastest.
Arguments:
- layer_input: bfloat16 [8, 1024, 2048], P(None, ('sp', 'tp')), may hold values from -6 to 6
- input_gain: float32 [2048], replicated, may hold values from 0.5 to 1.5
- narrowing_matrix: bfloat16 [2048, 512], replicated, may hold values from -0.125 to 0.125
- rotary_down: bfloat16 [2048, 64], replicated, may hold values from -0.125 to 0.125
- summary_scaling: float32 [512], replicated, may hold values from 0.5 to 1.5
- lookup_widening: bfloat16 [512, 16, 128], P('tp'), may hold values from -0.25 to 0.25
- payload_widening: bfloat16 [512, 16, 128], P('tp'), may hold values from -0.25 to 0.25
- query_nope: bfloat16 [8, 16, 128], P('sp', 'tp'), may hold values from -6 to 6
- query_rotary: bfloat16 [8, 16, 64], P('sp', 'tp'), may hold values from -6 to 6
Outputs:
- stored_summaries: bfloat16 [8, 1024, 512], P('sp', None, 'tp')
- rotary_cache: bfloat16 [8, 1024, 64], P('sp', None, 'tp')
- first_read: bfloat16 [8, 16, 128], P('sp', 'tp')
All inputs are finite; a program needn't handle non-finite values.
Results may differ from a plain program's by a relative error of at most 0.02.
Values may be sent and summed in bfloat16 or wider, within the bound.
A program may use at most 64 MiB of HBM per device.

v0:
```python
import jax
import jax.numpy as jnp
from jax import lax
from jax.sharding import PartitionSpec as P

QK_ROPE = 64
PLAIN_MATCH_SPAN = 128
norm_eps = 1e-06
rotary_base = 10000.0


def summed_rows(portion, width, axis):
    count = width * lax.axis_size(axis)
    return lax.psum_scatter(portion(jnp.int32(0), count), axis, scatter_dimension=0, tiled=True)


def rescaled_lines(vector):
    return vector * lax.rsqrt(jnp.mean(vector * vector, axis=-1, keepdims=True) + norm_eps)


def rotate(vector, position):
    half_width = vector.shape[-1] // 2
    frequency = 1.0 / rotary_base ** (
        jnp.arange(half_width, dtype=jnp.float32) * 2.0 / vector.shape[-1]
    )
    angles = position * frequency
    first_half = vector[..., :half_width]
    second_half = vector[..., half_width:]
    return jnp.concatenate(
        [
            first_half * jnp.cos(angles) - second_half * jnp.sin(angles),
            second_half * jnp.cos(angles) + first_half * jnp.sin(angles),
        ],
        axis=-1,
    )


def to_pieces(array, sp_count, tp_count):
    seq_count, pos_local, cache_width = array.shape
    seq_each = seq_count // sp_count
    width_each = cache_width // tp_count
    array = array.reshape(sp_count, seq_each, pos_local, tp_count, width_each)
    array = array.transpose(0, 3, 1, 2, 4)
    return array.reshape(sp_count * tp_count, seq_each, pos_local, width_each)


def shards(
    layer_input,
    input_gain,
    narrowing_matrix,
    rotary_down,
    summary_scaling,
    lookup_widening,
    payload_widening,
    query_nope,
    query_rotary,
):
    seq_count, pos_local, feature_width = layer_input.shape
    sp_count = lax.axis_size("sp")
    tp_count = lax.axis_size("tp")
    block_index = lax.axis_index(("sp", "tp"))
    normed = (rescaled_lines(layer_input.astype(jnp.float32)) * input_gain).astype(jnp.bfloat16)
    flat_rows = normed.reshape(seq_count * pos_local, feature_width)
    hidden_summary = jnp.dot(
        flat_rows, narrowing_matrix, preferred_element_type=jnp.float32
    ).astype(jnp.bfloat16)
    rotary = jnp.dot(flat_rows, rotary_down, preferred_element_type=jnp.float32).astype(
        jnp.bfloat16
    )
    hidden_summary = (
        (rescaled_lines(hidden_summary.astype(jnp.float32)) * summary_scaling)
        .astype(jnp.bfloat16)
        .reshape(seq_count, pos_local, -1)
    )
    positions = (block_index * pos_local + jnp.arange(pos_local, dtype=jnp.int32)).astype(
        jnp.float32
    )[None, :, None]
    rotary = rotate(rotary.astype(jnp.float32).reshape(seq_count, pos_local, -1), positions).astype(
        jnp.bfloat16
    )
    moved = (
        lax.all_to_all(
            to_pieces(hidden_summary, sp_count, tp_count),
            ("sp", "tp"),
            split_axis=0,
            concat_axis=2,
            tiled=True,
        ),
        lax.all_to_all(
            to_pieces(rotary, sp_count, tp_count),
            ("sp", "tp"),
            split_axis=0,
            concat_axis=2,
            tiled=True,
        ),
    )
    hidden_summary = moved[0][0]
    rotary = moved[1][0]
    pos_total = hidden_summary.shape[1]
    rot_each = rotary.shape[2]
    head_each = query_nope.shape[1]
    query_all, turn_all = (
        lax.all_gather(query_nope, "tp", axis=1, tiled=True),
        lax.all_gather(query_rotary, "tp", axis=1, tiled=True),
    )
    absorbed = jnp.einsum(
        "shd,chd->shc", query_all, lookup_widening, preferred_element_type=jnp.float32
    ).astype(jnp.bfloat16)
    query_turned = rotate(turn_all.astype(jnp.float32), jnp.float32(pos_total)).astype(jnp.bfloat16)
    turned_mine = lax.dynamic_slice_in_dim(
        query_turned, lax.axis_index("tp") * rot_each, rot_each, 2
    )
    score_scale = (PLAIN_MATCH_SPAN + QK_ROPE) ** (-0.5)
    partial_value = (
        jnp.einsum("shc,spc->shp", absorbed, hidden_summary, preferred_element_type=jnp.float32)
        + jnp.einsum("shr,spr->shp", turned_mine, rotary, preferred_element_type=jnp.float32)
    ) * score_scale
    scores = lax.psum(partial_value.astype(jnp.bfloat16), "tp").astype(jnp.float32)
    attention = jax.nn.softmax(scores, axis=-1).astype(jnp.bfloat16)
    context = jnp.einsum(
        "shp,spc->shc", attention, hidden_summary, preferred_element_type=jnp.float32
    ).astype(jnp.bfloat16)

    def project_heads(row_start, row_count):
        part_context = lax.dynamic_slice_in_dim(context, row_start, row_count, 1)
        part_weight = lax.dynamic_slice_in_dim(payload_widening, row_start, row_count, 1)
        return jnp.einsum(
            "shc,chv->hsv", part_context, part_weight, preferred_element_type=jnp.float32
        )

    values = summed_rows(project_heads, head_each, "tp")
    first_read = rescaled_lines(values.transpose(1, 0, 2)).astype(jnp.bfloat16)
    return (hidden_summary, rotary, first_read)


def solution(mesh):
    return jax.shard_map(
        shards,
        mesh=mesh,
        in_specs=(
            P(None, ("sp", "tp"), None),
            P(),
            P(),
            P(),
            P(),
            P("tp", None, None),
            P("tp", None, None),
            P("sp", "tp", None),
            P("sp", "tp", None),
        ),
        out_specs=(P("sp", None, "tp"), P("sp", None, "tp"), P("sp", "tp", None)),
        check_vma=False,
    )
```

profile of v0, /device:TPU:0, one launch (start us, length us, event | category | flops | bytes accessed | tf_op | source)
XLA Modules:
  0.0 55.6 jit_solution(11520406021461989264)
XLA Ops:
  0.6 0.0 copy-start
  0.6 0.0 copy-start.1
  0.7 1.7 %fusion = f32[8,32]{1,0:T(8,128)S(1)} fusion(bf16[8,32,2048]{2,1,0:T(8,128)(2,1)} %param.9), kind=kLoop, calls=%fused_computation.2 | loop fusion | flops 1572608 | bytes 1049600 | tf_op jit(solution)/shard_map/reduce_sum | solution.py:18
  2.4 1.5 %fusion.2 = bf16[8,32,2048]{2,1,0:T(8,128)(2,1)S(1)} fusion(bf16[8,32,2048]{2,1,0:T(8,128)(2,1)} %param.9, f32[2048]{0:T(1024)} %param.10, f32[8,32]{1,0:T(8,128)S(1)} %add_rsqrt_fusion), kind=kLoop, calls=%fused_computation.4 | loop fusion | flops 2097152 | bytes 2106368 | tf_op jit(solution)/shard_map/convert_element_type | solution.py:62
  3.9 0.0 copy-done.1
  4.0 0.4 fusion.6
  4.4 0.1 copy.33
  4.5 0.1 multiply_cosine_fusion
  4.6 0.1 subtract_convert_fusion
  4.8 0.1 pad_maximum_fusion
  4.9 0.1 copy.34
  5.0 0.0 copy-start.2
  5.0 0.8 %reshape.300 = bf16[32,2,256]{2,1,0:T(2,128)(2,1)} reshape(bf16[32,1,16,32]{3,2,1,0:T(8,128)(2,1)S(1)} %bitcast.62) | data formatting | bytes 65536
  5.8 7.3 %all-to-all-start.1 = ((bf16[32,2,256]{2,1,0:T(2,128)(2,1)}), bf16[32,2,256]{2,1,0:T(2,128)(2,1)S(1)}, u32[]{:S(2)}, u32[]{:S(2)}) async-start(bf16[32,2,256]{2,1,0:T(2,128)(2,1)} %reshape.300), calls=%async_computation.1 | async-start | bytes 65536 | tf_op jit(solution)/shard_map/all_to_all | solution.py:89
  13.1 0.0 copy-done.3
  13.1 5.2 %all_gather.7 = bf16[1,16,64]{2,0,1:T(2,128)(2,1)S(1)} all-gather(bf16[1,4,64]{2,0,1:T(2,128)(2,1)S(1)} %copy.37), channel_id=1, replica_groups=mesh['sp'=8,'tp'=4] {'tp'}, dimensions={1}, use_global_device_ids=true | all-gather | bytes 2560 | tf_op jit(solution)/shard_map/all_gather | solution.py:104
  18.3 0.0 copy-done
  18.3 0.8 %multiply_reduce_fusion = (f32[256]{0:T(256)S(1)}, f32[256,512]{1,0:T(8,128)S(1)}) fusion(bf16[256,2048]{1,0:T(8,128)(2,1)S(1)} %bitcast.57, bf16[2048,512]{1,0:T(8,128)(2,1)S(1)} %copy-done), kind=kOutput, calls=%fused_computation.20 | convolution fusion | flops 537394944 | bytes 3671040 | tf_op jit(solution)/shard_map/dot_general | solution.py:64
  19.1 0.0 copy-start.4
  19.1 0.0 copy-start.7
  19.1 0.0 copy-start.5
  19.2 0.0 copy-done.2
  19.2 0.1 multiply_convert_fusion
  19.3 0.1 reshape_reshape.3
  19.4 0.0 copy-start.6
  19.4 0.8 %copy.31 = bf16[8,1,32,4,128]{4,2,3,0,1:T(8,128)(2,1)} copy(bf16[8,1,32,4,128]{4,3,2,0,1:T(4,128)(2,1)S(1)} %reshape_reshape.3) | data formatting | bytes 524288 | tf_op jit(solution)/shard_map/reshape;reshape | solution.py:42
  20.1 0.2 all-to-all-done.1
  20.4 5.6 %all-to-all-start = ((bf16[32,1,32,128]{3,2,1,0:T(8,128)(2,1)}), bf16[32,1,32,128]{3,2,1,0:T(8,128)(2,1)S(1)}, u32[]{:S(2)}, u32[]{:S(2)}) async-start(bf16[32,1,32,128]{3,2,1,0:T(8,128)(2,1)} %bitcast.3), calls=%async_computation | async-start | bytes 524288 | tf_op jit(solution)/shard_map/all_to_all | solution.py:82
  26.1 0.6 %dynamic-slice = u32[1]{0:T(128)} dynamic-slice(u32[32]{0:T(128)S(1)} %copy-done.7, u32[]{:T(128)S(6)} %add.73), dynamic_slice_sizes={1} | dynamic-slice | bytes 12
  27.3 5.2 %all_gather.6 = bf16[1,16,128]{2,0,1:T(2,128)(2,1)S(1)} all-gather(bf16[1,4,128]{2,0,1:T(2,128)(2,1)S(1)} %copy.36), channel_id=1, replica_groups=mesh['sp'=8,'tp'=4] {'tp'}, dimensions={1}, use_global_device_ids=true | all-gather | bytes 5120 | tf_op jit(solution)/shard_map/all_gather | solution.py:103
  32.5 0.1 subtract_convert_fusion.1
  32.6 0.4 fusion.11
  33.0 0.2 reshape.301
  33.2 0.2 reshape.287
  33.3 0.8 %squeeze.7 = bf16[1,1024,16]{1,2,0:T(8,128)(2,1)} reshape(bf16[32,1,32,16]{2,0,3,1:T(8,128)(2,1)S(1)} %copy.35) | data formatting | bytes 65536 | tf_op jit(solution)/shard_map/squeeze | solution.py:98
  34.1 2.4 %all-to-all-done = bf16[32,1,32,128]{3,2,1,0:T(8,128)(2,1)S(1)} async-done(((bf16[32,1,32,128]{3,2,1,0:T(8,128)(2,1)}), bf16[32,1,32,128]{3,2,1,0:T(8,128)(2,1)S(1)}, u32[]{:S(2)}, u32[]{:S(2)}) %all-to-all-start) | async-done | bytes 262176 | tf_op jit(solution)/shard_map/all_to_all | solution.py:82
  36.5 0.2 fusion.25
  36.7 0.2 fusion.7
  36.9 10.6 %psum.7 = bf16[1,16,1024]{2,1,0:T(8,128)(2,1)S(1)} all-reduce(bf16[1,16,1024]{2,1,0:T(8,128)(2,1)S(1)} %fusion.7), channel_id=1, replica_groups=mesh['sp'=8,'tp'=4] {'tp'}, use_global_device_ids=true, to_apply=%region_2.0 | all-reduce | flops 16384 | bytes 65536 | tf_op jit(solution)/shard_map/psum | solution.py:118
  47.5 0.1 reduce_max.14
  47.7 0.2 fusion.13
  47.9 0.2 fusion.8
  48.1 0.0 copy-done.6
  48.1 0.3 fusion.9
  48.3 5.8 %all-reduce = f32[16,1,128]{2,0,1:T(8,128)S(1)} all-reduce(f32[16,1,128]{2,0,1:T(8,128)S(1)} %bitcast.64), channel_id=2, replica_groups=mesh['sp'=8,'tp'=4] {'tp'}, use_global_device_ids=true, to_apply=%region_5.0.clone | all-reduce | flops 2048 | bytes 16384
  54.1 0.1 multiply_reduce_fusion.1
  54.2 0.6 %multiply_convert_fusion.1 = bf16[1,4,128]{2,1,0:T(4,128)(2,1)} fusion(f32[16,1,128]{2,0,1:T(8,128)S(1)} %all-reduce, u32[]{:T(128)S(6)} %multiply.33, f32[4]{0:T(128)S(1)} %add_rsqrt_fusion.2), kind=kLoop, calls=%fused_computation.46 | loop fusion | flops 1024 | bytes 3092 | tf_op jit(solution)/shard_map/convert_element_type | solution.py:132
  54.9 0.7 %copy.56 = bf16[1,1024,128]{2,1,0:T(8,128)(2,1)} copy(bf16[1,1024,128]{2,1,0:T(8,128)(2,1)S(1)} %bitcast.60) | data formatting | bytes 524288
  (15 shorter events, 0.1 us)
Async XLA Ops:
  0.6 17.7 %copy-start = (bf16[2048,512]{1,0:T(8,128)(2,1)S(1)}, bf16[2048,512]{1,0:T(8,128)(2,1)}, u32[]{:S(2)}) copy-start(bf16[2048,512]{1,0:T(8,128)(2,1)} %param.11) | copy-start | bytes 6291460
  0.6 3.3 %copy-start.1 = (bf16[2048,64]{0,1:T(8,128)(2,1)S(1)}, bf16[2048,64]{0,1:T(8,128)(2,1)}, u32[]{:S(2)}) copy-start(bf16[2048,64]{0,1:T(8,128)(2,1)} %param.12) | copy-start | bytes 786436
  2.4 10.7 %copy-start.3 = (bf16[1,4,64]{2,1,0:T(4,128)(2,1)S(1)}, bf16[1,4,64]{2,1,0:T(4,128)(2,1)}, u32[]{:S(2)}) copy-start(bf16[1,4,64]{2,1,0:T(4,128)(2,1)} %param.17) | copy-start | bytes 1540
  5.0 14.2 %copy-start.2 = (f32[512]{0:T(512)S(1)}, f32[512]{0:T(512)}, u32[]{:S(2)}) copy-start(f32[512]{0:T(512)} %param.13) | copy-start | bytes 6148
  5.8 14.6 %all-to-all-start.1 = ((bf16[32,2,256]{2,1,0:T(2,128)(2,1)}), bf16[32,2,256]{2,1,0:T(2,128)(2,1)S(1)}, u32[]{:S(2)}, u32[]{:S(2)}) async-start(bf16[32,2,256]{2,1,0:T(2,128)(2,1)} %reshape.300), calls=%async_computation.1 | async-start | bytes 65536 | tf_op jit(solution)/shard_map/all_to_all | solution.py:89
  19.1 6.9 %copy-start.4 = (bf16[1,4,128]{2,1,0:T(4,128)(2,1)S(1)}, bf16[1,4,128]{2,1,0:T(4,128)(2,1)}, u32[]{:S(2)}) copy-start(bf16[1,4,128]{2,1,0:T(4,128)(2,1)} %param.16) | copy-start | bytes 3076
  19.1 7.0 %copy-start.7 = (u32[32]{0:T(128)S(1)}, u32[32]{0:T(128)}, u32[]{:S(2)}) copy-start(u32[32]{0:T(128)} %constant.54) | copy-start | bytes 388
  19.1 13.5 %copy-start.5 = (bf16[128,16,128]{2,1,0:T(8,128)(2,1)S(1)}, bf16[128,16,128]{2,1,0:T(8,128)(2,1)}, u32[]{:S(2)}) copy-start(bf16[128,16,128]{2,1,0:T(8,128)(2,1)} %param.14) | copy-start | bytes 1572868
  19.4 28.7 %copy-start.6 = (bf16[128,16,128]{2,1,0:T(8,128)(2,1)S(1)}, bf16[128,16,128]{2,1,0:T(8,128)(2,1)}, u32[]{:S(2)}) copy-start(bf16[128,16,128]{2,1,0:T(8,128)(2,1)} %param.15) | copy-start | bytes 1572868
  20.4 16.2 %all-to-all-start = ((bf16[32,1,32,128]{3,2,1,0:T(8,128)(2,1)}), bf16[32,1,32,128]{3,2,1,0:T(8,128)(2,1)S(1)}, u32[]{:S(2)}, u32[]{:S(2)}) async-start(bf16[32,1,32,128]{3,2,1,0:T(8,128)(2,1)} %bitcast.3), calls=%async_computation | async-start | bytes 524288 | tf_op jit(solution)/shard_map/all_to_all | solution.py:82
where the time goes:
time: 55.9 us; the launch traced here: 55.6 us
  blocking collectives  26.7 us (48%)
  starting transfers between devices  12.9 us (23%)
  other arithmetic  4.95 us (9%)
  local copies, waits for them, and re-layouts  4.3 us (8%)
  waiting for transfers between devices  2.64 us (5%)
  matrix products  2.46 us (4%)
  between operations  1.56 us (3%)
    psum x1, blocking collectives, shards(): lax.psum(partial_value.astype(jnp.bfloat16), 'tp').astype(jnp.float32)  10.6 us
    all_to_all x1, starting transfers between devices, shards(): lax.all_to_all(to_pieces(rotary, sp_count, tp_count), ('sp', 'tp'), split...  7.33 us
    unnamed x1, blocking collectives  5.76 us
    all_to_all x1, starting transfers between devices, shards(): lax.all_to_all(to_pieces(hidden_summary, sp_count, tp_count), ('sp', 'tp'...  5.61 us
    all_gather x1, blocking collectives, shards(): lax.all_gather(query_nope, 'tp', axis=1, tiled=True)  5.2 us
    all_gather x1, blocking collectives, shards(): lax.all_gather(query_rotary, 'tp', axis=1, tiled=True)  5.19 us
    all_to_all x1, waiting for transfers between devices, shards(): lax.all_to_all(to_pieces(hidden_summary, sp_count, tp_count), ('sp', 'tp'...  2.41 us
    unnamed x22, local copies, waits for them, and re-layouts  2.26 us
  transfers between devices with their start and end apart: 2, of which 2 were waited for; matrix products, arithmetic and copies ran while one was open for 7% of the time, Pallas kernels for 0%

commit v1 on v0

--- a/solution.py
+++ b/solution.py
@@ -115,7 +115,9 @@
         jnp.einsum("shc,spc->shp", absorbed, hidden_summary, preferred_element_type=jnp.float32)
         + jnp.einsum("shr,spr->shp", turned_mine, rotary, preferred_element_type=jnp.float32)
     ) * score_scale
-    scores = lax.psum(partial_value.astype(jnp.bfloat16), "tp").astype(jnp.float32)
+    scores = jnp.sum(lax.all_gather(partial_value.astype(jnp.bfloat16), "tp"), axis=0).astype(
+        jnp.float32
+    )
     attention = jax.nn.softmax(scores, axis=-1).astype(jnp.bfloat16)
     context = jnp.einsum(
         "shp,spc->shc", attention, hidden_summary, preferred_element_type=jnp.float32

time: 55.9 us -> 51.1 us (0.914)
  blocking collectives: 26.7 us -> 21.9 us
    psum x1 -> x0, blocking collectives: 10.6 us -> none  [shards(): lax.psum(partial_value.astype(jnp.bfloat16), 'tp').astype(jnp.float32)]
    all_gather x0 -> x1, blocking collectives: none -> 5.41 us  [shards(): lax.all_gather(partial_value.astype(jnp.bfloat16), 'tp')]
  transfers between devices with their start and end apart: 2 -> 2, of which waited for: 2 -> 2; matrix products, arithmetic and copies ran while one was open for 7% -> 8% of each run, Pallas kernels for 0% -> 0%
where the time goes in v1:
time: 51.1 us; the launch traced here: 50.8 us
  blocking collectives  21.9 us (43%)
  starting transfers between devices  12.9 us (25%)
  other arithmetic  4.97 us (10%)
  local copies, waits for them, and re-layouts  4.3 us (8%)
  waiting for transfers between devices  2.64 us (5%)
  matrix products  2.46 us (5%)
  between operations  1.56 us (3%)
    all_to_all x1, starting transfers between devices, shards(): lax.all_to_all(to_pieces(rotary, sp_count, tp_count), ('sp', 'tp'), split...  7.33 us
    unnamed x1, blocking collectives  6.08 us
    all_to_all x1, starting transfers between devices, shards(): lax.all_to_all(to_pieces(hidden_summary, sp_count, tp_count), ('sp', 'tp'...  5.61 us
    all_gather x1, blocking collectives, shards(): lax.all_gather(partial_value.astype(jnp.bfloat16), 'tp')  5.41 us
    all_gather x1, blocking collectives, shards(): lax.all_gather(query_nope, 'tp', axis=1, tiled=True)  5.2 us
    all_gather x1, blocking collectives, shards(): lax.all_gather(query_rotary, 'tp', axis=1, tiled=True)  5.19 us
    all_to_all x1, waiting for transfers between devices, shards(): lax.all_to_all(to_pieces(hidden_summary, sp_count, tp_count), ('sp', 'tp'...  2.41 us
    unnamed x22, local copies, waits for them, and re-layouts  2.26 us
  transfers between devices with their start and end apart: 2, of which 2 were waited for; matrix products, arithmetic and copies ran while one was open for 8% of the time, Pallas kernels for 0%

profile of v1, /device:TPU:0, one launch (start us, length us, event | category | flops | bytes accessed | tf_op | source)
XLA Modules:
  0.0 50.8 jit_solution(15715659774731488801)
XLA Ops:
  0.6 0.0 copy-start
  0.6 0.0 copy-start.1
  0.7 1.7 %fusion = f32[8,32]{1,0:T(8,128)S(1)} fusion(bf16[8,32,2048]{2,1,0:T(8,128)(2,1)} %param.9), kind=kLoop, calls=%fused_computation.2 | loop fusion | flops 1572608 | bytes 1049600 | tf_op jit(solution)/shard_map/reduce_sum | solution.py:18
  2.4 1.5 %fusion.2 = bf16[8,32,2048]{2,1,0:T(8,128)(2,1)S(1)} fusion(bf16[8,32,2048]{2,1,0:T(8,128)(2,1)} %param.9, f32[2048]{0:T(1024)} %param.10, f32[8,32]{1,0:T(8,128)S(1)} %add_rsqrt_fusion), kind=kLoop, calls=%fused_computation.4 | loop fusion | flops 2097152 | bytes 2106368 | tf_op jit(solution)/shard_map/convert_element_type | solution.py:62
  3.9 0.0 copy-done.1
  4.0 0.4 fusion.6
  4.4 0.1 copy.42
  4.5 0.1 multiply_cosine_fusion
  4.6 0.1 subtract_convert_fusion
  4.8 0.1 pad_maximum_fusion
  4.9 0.1 copy.43
  5.0 0.0 copy-start.2
  5.0 0.8 %reshape.407 = bf16[32,2,256]{2,1,0:T(2,128)(2,1)} reshape(bf16[32,1,16,32]{3,2,1,0:T(8,128)(2,1)S(1)} %bitcast.83) | data formatting | bytes 65536
  5.8 7.3 %all-to-all-start.1 = ((bf16[32,2,256]{2,1,0:T(2,128)(2,1)}), bf16[32,2,256]{2,1,0:T(2,128)(2,1)S(1)}, u32[]{:S(2)}, u32[]{:S(2)}) async-start(bf16[32,2,256]{2,1,0:T(2,128)(2,1)} %reshape.407), calls=%async_computation.1 | async-start | bytes 65536 | tf_op jit(solution)/shard_map/all_to_all | solution.py:89
  13.1 0.0 copy-done.3
  13.1 5.2 %all_gather.13 = bf16[1,16,64]{2,0,1:T(2,128)(2,1)S(1)} all-gather(bf16[1,4,64]{2,0,1:T(2,128)(2,1)S(1)} %copy.46), channel_id=1, replica_groups=mesh['sp'=8,'tp'=4] {'tp'}, dimensions={1}, use_global_device_ids=true | all-gather | bytes 2560 | tf_op jit(solution)/shard_map/all_gather | solution.py:104
  18.3 0.0 copy-done
  18.3 0.8 %multiply_reduce_fusion = (f32[256]{0:T(256)S(1)}, f32[256,512]{1,0:T(8,128)S(1)}) fusion(bf16[256,2048]{1,0:T(8,128)(2,1)S(1)} %bitcast.77, bf16[2048,512]{1,0:T(8,128)(2,1)S(1)} %copy-done), kind=kOutput, calls=%fused_computation.19 | convolution fusion | flops 537394944 | bytes 3671040 | tf_op jit(solution)/shard_map/dot_general | solution.py:64
  19.1 0.0 copy-start.4
  19.1 0.0 copy-start.7
  19.1 0.0 copy-start.5
  19.2 0.0 copy-done.2
  19.2 0.1 multiply_convert_fusion
  19.3 0.1 reshape_reshape.3
  19.4 0.0 copy-start.6
  19.4 0.8 %copy.40 = bf16[8,1,32,4,128]{4,2,3,0,1:T(8,128)(2,1)} copy(bf16[8,1,32,4,128]{4,3,2,0,1:T(4,128)(2,1)S(1)} %reshape_reshape.3) | data formatting | bytes 524288 | tf_op jit(solution)/shard_map/reshape;reshape | solution.py:42
  20.1 0.2 all-to-all-done.1
  20.4 5.6 %all-to-all-start = ((bf16[32,1,32,128]{3,2,1,0:T(8,128)(2,1)}), bf16[32,1,32,128]{3,2,1,0:T(8,128)(2,1)S(1)}, u32[]{:S(2)}, u32[]{:S(2)}) async-start(bf16[32,1,32,128]{3,2,1,0:T(8,128)(2,1)} %bitcast.3), calls=%async_computation | async-start | bytes 524288 | tf_op jit(solution)/shard_map/all_to_all | solution.py:82
  26.0 0.0 copy-done.4
  26.1 0.6 %dynamic-slice = u32[1]{0:T(128)} dynamic-slice(u32[32]{0:T(128)S(1)} %copy-done.7, u32[]{:T(128)S(6)} %add.71), dynamic_slice_sizes={1} | dynamic-slice | bytes 12
  27.3 5.2 %all_gather.12 = bf16[1,16,128]{2,0,1:T(2,128)(2,1)S(1)} all-gather(bf16[1,4,128]{2,0,1:T(2,128)(2,1)S(1)} %copy.45), channel_id=1, replica_groups=mesh['sp'=8,'tp'=4] {'tp'}, dimensions={1}, use_global_device_ids=true | all-gather | bytes 5120 | tf_op jit(solution)/shard_map/all_gather | solution.py:103
  32.5 0.1 subtract_convert_fusion.1
  32.6 0.4 fusion.10
  33.0 0.2 reshape.408
  33.2 0.2 reshape.391
  33.3 0.8 %squeeze.7 = bf16[1,1024,16]{1,2,0:T(8,128)(2,1)} reshape(bf16[32,1,32,16]{2,0,3,1:T(8,128)(2,1)S(1)} %copy.44) | data formatting | bytes 65536 | tf_op jit(solution)/shard_map/squeeze | solution.py:98
  34.1 2.4 %all-to-all-done = bf16[32,1,32,128]{3,2,1,0:T(8,128)(2,1)S(1)} async-done(((bf16[32,1,32,128]{3,2,1,0:T(8,128)(2,1)}), bf16[32,1,32,128]{3,2,1,0:T(8,128)(2,1)S(1)}, u32[]{:S(2)}, u32[]{:S(2)}) %all-to-all-start) | async-done | bytes 262176 | tf_op jit(solution)/shard_map/all_to_all | solution.py:82
  36.5 0.2 fusion.30
  36.7 0.2 fusion.5
  36.9 5.4 %all-gather = bf16[64,1024]{1,0:T(8,128)(2,1)S(1)} all-gather(bf16[16,1024]{1,0:T(8,128)(2,1)S(1)} %fusion.5), channel_id=2, replica_groups=mesh['sp'=8,'tp'=4] {'tp'}, dimensions={0}, use_global_device_ids=true | all-gather | bytes 163840 | tf_op jit(solution)/shard_map/all_gather | solution.py:118
  42.4 0.1 reduce_max.14
  42.5 0.2 fusion.18
  42.7 0.2 fusion.7
  42.9 0.3 fusion.8
  43.2 6.1 %all-reduce = f32[16,1,128]{2,0,1:T(8,128)S(1)} all-reduce(f32[16,1,128]{2,0,1:T(8,128)S(1)} %bitcast.85), channel_id=3, replica_groups=mesh['sp'=8,'tp'=4] {'tp'}, use_global_device_ids=true, to_apply=%region_5.0.clone | all-reduce | flops 2048 | bytes 16384
  49.3 0.1 multiply_reduce_fusion.1
  49.4 0.6 %multiply_convert_fusion.1 = bf16[1,4,128]{2,1,0:T(4,128)(2,1)} fusion(f32[16,1,128]{2,0,1:T(8,128)S(1)} %all-reduce, u32[]{:T(128)S(6)} %multiply.33, f32[4]{0:T(128)S(1)} %add_rsqrt_fusion.2), kind=kLoop, calls=%fused_computation.51 | loop fusion | flops 1024 | bytes 3092 | tf_op jit(solution)/shard_map/convert_element_type | solution.py:134
  50.0 0.7 %copy.65 = bf16[1,1024,128]{2,1,0:T(8,128)(2,1)} copy(bf16[1,1024,128]{2,1,0:T(8,128)(2,1)S(1)} %bitcast.80) | data formatting | bytes 524288
  (16 shorter events, 0.2 us)
Async XLA Ops:
  0.6 17.7 %copy-start = (bf16[2048,512]{1,0:T(8,128)(2,1)S(1)}, bf16[2048,512]{1,0:T(8,128)(2,1)}, u32[]{:S(2)}) copy-start(bf16[2048,512]{1,0:T(8,128)(2,1)} %param.11) | copy-start | bytes 6291460
  0.6 3.3 %copy-start.1 = (bf16[2048,64]{0,1:T(8,128)(2,1)S(1)}, bf16[2048,64]{0,1:T(8,128)(2,1)}, u32[]{:S(2)}) copy-start(bf16[2048,64]{0,1:T(8,128)(2,1)} %param.12) | copy-start | bytes 786436
  2.4 10.7 %copy-start.3 = (bf16[1,4,64]{2,1,0:T(4,128)(2,1)S(1)}, bf16[1,4,64]{2,1,0:T(4,128)(2,1)}, u32[]{:S(2)}) copy-start(bf16[1,4,64]{2,1,0:T(4,128)(2,1)} %param.17) | copy-start | bytes 1540
  5.0 14.2 %copy-start.2 = (f32[512]{0:T(512)S(1)}, f32[512]{0:T(512)}, u32[]{:S(2)}) copy-start(f32[512]{0:T(512)} %param.13) | copy-start | bytes 6148
  5.8 14.6 %all-to-all-start.1 = ((bf16[32,2,256]{2,1,0:T(2,128)(2,1)}), bf16[32,2,256]{2,1,0:T(2,128)(2,1)S(1)}, u32[]{:S(2)}, u32[]{:S(2)}) async-start(bf16[32,2,256]{2,1,0:T(2,128)(2,1)} %reshape.407), calls=%async_computation.1 | async-start | bytes 65536 | tf_op jit(solution)/shard_map/all_to_all | solution.py:89
  19.1 6.9 %copy-start.4 = (bf16[1,4,128]{2,1,0:T(4,128)(2,1)S(1)}, bf16[1,4,128]{2,1,0:T(4,128)(2,1)}, u32[]{:S(2)}) copy-start(bf16[1,4,128]{2,1,0:T(4,128)(2,1)} %param.16) | copy-start | bytes 3076
  19.1 7.0 %copy-start.7 = (u32[32]{0:T(128)S(1)}, u32[32]{0:T(128)}, u32[]{:S(2)}) copy-start(u32[32]{0:T(128)} %constant.56) | copy-start | bytes 388
  19.1 13.5 %copy-start.5 = (bf16[128,16,128]{2,1,0:T(8,128)(2,1)S(1)}, bf16[128,16,128]{2,1,0:T(8,128)(2,1)}, u32[]{:S(2)}) copy-start(bf16[128,16,128]{2,1,0:T(8,128)(2,1)} %param.14) | copy-start | bytes 1572868
  19.4 23.6 %copy-start.6 = (bf16[128,16,128]{2,1,0:T(8,128)(2,1)S(1)}, bf16[128,16,128]{2,1,0:T(8,128)(2,1)}, u32[]{:S(2)}) copy-start(bf16[128,16,128]{2,1,0:T(8,128)(2,1)} %param.15) | copy-start | bytes 1572868
  20.4 16.2 %all-to-all-start = ((bf16[32,1,32,128]{3,2,1,0:T(8,128)(2,1)}), bf16[32,1,32,128]{3,2,1,0:T(8,128)(2,1)S(1)}, u32[]{:S(2)}, u32[]{:S(2)}) async-start(bf16[32,1,32,128]{3,2,1,0:T(8,128)(2,1)} %bitcast.3), calls=%async_computation | async-start | bytes 524288 | tf_op jit(solution)/shard_map/all_to_all | solution.py:82
